TPU v7x, 32 devices: a whole 2x2x4 slice. The times are simulated.
32 devices in a mesh: fs: 8 (over z, x), tp: 4 (over y, core).
Axes of the slice: x: 2, y: 2, z: 4, core: 2. Of those that a mesh axis runs over, the one named last changes fastest.
Arguments:
- tokens: bfloat16 [2048, 1536], P('fs', 'tp'), may hold values from -6 to 6
- norm_in_gain: float32 [1536], replicated, may hold values from 0.1 to 1.9
- query_w: bfloat16 [1536, 768], P('fs', 'tp'), may hold values from -0.15625 to 0.15625
- key_w: bfloat16 [1536, 768], P('fs', 'tp'), may hold values from -0.15625 to 0.15625
- value_w: bfloat16 [1536, 768], P('fs', 'tp'), may hold values from -0.15625 to 0.15625
- gate_w: bfloat16 [1536, 768], P('fs', 'tp'), may hold values from -0.15625 to 0.15625
- out_w: bfloat16 [768, 1536], P('tp', 'fs'), may hold values from -0.21875 to 0.21875
- norm_mid_gain: float32 [1536], replicated, may hold values from 0.1 to 1.9
- up_gate_w: bfloat16 [1536, 4096], P('fs', 'tp'), may hold values from -0.15625 to 0.15625
- up_value_w: bfloat16 [1536, 4096], P('fs', 'tp'), may hold values from -0.15625 to 0.15625
- conv_taps: float32 [3, 4096], P(None, 'tp'), may hold values from -3.5 to 3.5
- conv_bias: float32 [4096], P('tp'), may hold values from -3 to 3
- down_w: bfloat16 [4096, 1536], P('tp', 'fs'), may hold values from -0.09375 to 0.09375
Outputs:
- layer_out: bfloat16 [2048, 1536], P('fs', 'tp')
All inputs are finite; a program needn't handle non-finite values.
Results may differ from a plain program's by a relative error of at most 0.02.
Values may be sent and summed in bfloat16 or wider, within the bound.
A program may use at most 64 MiB of HBM per device.

v0:
```python
import jax
import jax.numpy as jnp
from jax import lax
from jax.sharding import PartitionSpec as P

BLOCK = 32
HEAD_DIM = 96


epsilon = 1e-06
rotary_base = 10000.0


def taken_in(shard, axis, dim, absorb, state):
    everything = jax.tree.map(lambda a: lax.all_gather(a, axis, axis=dim, tiled=True), shard)
    return absorb(state, everything, jnp.int32(0))


def gathered_then(shard, axis, dim, block):
    whole = lax.all_gather(shard, axis, axis=dim, tiled=True)
    return block(whole, jnp.int32(0))


def rms_scale(row_block, gain_row):
    widened = row_block.astype(jnp.float32)
    scaled = widened * lax.rsqrt(jnp.mean(widened * widened, axis=-1, keepdims=True) + epsilon)
    return (scaled * gain_row).astype(jnp.bfloat16)


def rotate(values_in, positions):
    half_width = values_in.shape[-1] // 2
    inv_freq = jnp.power(rotary_base, -jnp.arange(half_width, dtype=jnp.float32) / half_width)
    angles = positions[:, None] * inv_freq[None, :]
    cosine = jnp.cos(angles)[:, None, :]
    sine = jnp.sin(angles)[:, None, :]
    widened = values_in.astype(jnp.float32)
    first_half = widened[..., :half_width]
    second_half = widened[..., half_width:]
    return jnp.concatenate(
        [first_half * cosine - second_half * sine, first_half * sine + second_half * cosine],
        axis=-1,
    )


def retain(query_h, key_h, value_h, log_gamma, block_size):
    length, head_count, head_width = query_h.shape
    blocks = length // block_size
    offsets = jnp.arange(block_size, dtype=jnp.float32)
    lag_grid = offsets[:, None] - offsets[None, :]
    intra_decay = jnp.where(
        lag_grid[None] >= 0,
        jnp.exp(log_gamma[:, None, None] * jnp.maximum(lag_grid, 0.0)[None]),
        0.0,
    )
    query_decay = jnp.exp(log_gamma[None, :] * (offsets + 1.0)[:, None])
    key_decay = jnp.exp(log_gamma[None, :] * (block_size - 1.0 - offsets)[:, None])
    block_decay = jnp.exp(log_gamma * block_size)
    query_b = query_h.astype(jnp.float32).reshape(blocks, block_size, head_count, head_width)
    key_b = key_h.astype(jnp.float32).reshape(blocks, block_size, head_count, head_width)
    value_b = value_h.astype(jnp.float32).reshape(blocks, block_size, head_count, head_width)
    scores = (
        jnp.einsum("nchd,nshd->nhcs", query_b, key_b, precision=lax.Precision.HIGHEST)
        * intra_decay[None]
    )
    within = jnp.einsum("nhcs,nshe->nche", scores, value_b, precision=lax.Precision.HIGHEST)

    def advance(memory, block_inputs):
        query_n, key_n, value_n = block_inputs
        across_n = jnp.einsum(
            "chd,hde->che",
            query_n * query_decay[:, :, None],
            memory,
            precision=lax.Precision.HIGHEST,
        )
        memory = memory * block_decay[:, None, None] + jnp.einsum(
            "chd,che->hde", key_n * key_decay[:, :, None], value_n, precision=lax.Precision.HIGHEST
        )
        return (memory, across_n)

    initial = jnp.zeros((head_count, head_width, head_width), jnp.float32)
    final_memory, across = lax.scan(advance, initial, (query_b, key_b, value_b))
    return (within + across).reshape(length, head_count, head_width)


def mix_heads(queries, key_m, value_m, gate_m, log_gamma, head_width, block_size):
    length = queries.shape[0]
    head_count = queries.shape[1] // head_width
    positions = jnp.arange(length, dtype=jnp.float32)
    query_r = rotate(queries.reshape(length, head_count, head_width), positions).astype(
        jnp.bfloat16
    )
    key_r = (
        rotate(key_m.reshape(length, head_count, head_width), positions) * head_width ** (-0.5)
    ).astype(jnp.bfloat16)
    retained = retain(
        query_r, key_r, value_m.reshape(length, head_count, head_width), log_gamma, block_size
    )
    normed = retained * lax.rsqrt(jnp.mean(retained * retained, axis=-1, keepdims=True) + epsilon)
    return (normed.reshape(length, -1) * jax.nn.silu(gate_m.astype(jnp.float32))).astype(
        jnp.bfloat16
    )


def convolve(gate_up, conv_taps, conv_bias):
    length = gate_up.shape[0]
    tap_count = conv_taps.shape[0]
    padded = jnp.pad(gate_up.astype(jnp.float32), ((tap_count - 1, 0), (0, 0)))
    summed = jnp.zeros(gate_up.shape, jnp.float32) + conv_bias[None, :]
    for tap_index in range(tap_count):
        summed = summed + padded[tap_index : tap_index + length] * conv_taps[tap_index][None, :]
    return summed


def single(normed):

    def add_single(running, weight_piece, row_start):
        columns = lax.dynamic_slice_in_dim(normed, row_start, weight_piece.shape[0], 1)
        return running + jnp.dot(columns, weight_piece, preferred_element_type=jnp.float32)

    return add_single


def features(shard):
    return lax.all_gather(shard, "tp", axis=1, tiled=True)


def head_sum(terms):
    return lax.psum_scatter(
        terms.astype(jnp.bfloat16), "tp", scatter_dimension=1, tiled=True
    ).astype(jnp.float32)


def local(
    tokens,
    norm_in_gain,
    query_w,
    key_w,
    value_w,
    gate_w,
    out_w,
    norm_mid_gain,
    up_gate_w,
    up_value_w,
    conv_taps,
    conv_bias,
    down_w,
):
    normed_in = rms_scale(features(tokens), norm_in_gain)
    length = normed_in.shape[0]

    def empty(weight):
        return jnp.zeros((length, weight.shape[1]), jnp.float32)

    add_in = single(normed_in)

    def mixer_row(weight):
        return taken_in(weight, "fs", 0, add_in, empty(weight))

    queries = mixer_row(query_w)
    key_m = mixer_row(key_w)
    value_m = mixer_row(value_w)
    gate_m = mixer_row(gate_w)
    head_count = query_w.shape[1] // HEAD_DIM
    first_head = lax.axis_index("tp") * head_count
    head_ids = (first_head + jnp.arange(head_count, dtype=jnp.int32)).astype(jnp.float32)
    log_gamma = jnp.log1p(-jnp.exp2(-5.0 - head_ids))
    gated_heads = mix_heads(
        queries.astype(jnp.bfloat16),
        key_m.astype(jnp.bfloat16),
        value_m.astype(jnp.bfloat16),
        gate_m.astype(jnp.bfloat16),
        log_gamma,
        HEAD_DIM,
        BLOCK,
    )

    def mixer_project(weight_piece, row_start):
        return jnp.dot(gated_heads, weight_piece, preferred_element_type=jnp.float32)

    mixer_terms = gathered_then(out_w, "fs", 1, mixer_project)
    middle = (tokens.astype(jnp.float32) + head_sum(mixer_terms)).astype(jnp.bfloat16)
    normed_mid = rms_scale(features(middle), norm_mid_gain)
    add_mid = single(normed_mid)

    def channel_row(weight):
        return taken_in(weight, "fs", 0, add_mid, empty(weight))

    gate_up = channel_row(up_gate_w)
    value_up = channel_row(up_value_w)
    convolved = convolve(gate_up.astype(jnp.bfloat16), conv_taps, conv_bias)
    hidden = (jax.nn.silu(convolved) * value_up.astype(jnp.bfloat16).astype(jnp.float32)).astype(
        jnp.bfloat16
    )

    def channel_project(weight_piece, row_start):
        return jnp.dot(hidden, weight_piece, preferred_element_type=jnp.float32)

    channel_terms = gathered_then(down_w, "fs", 1, channel_project)
    return (middle.astype(jnp.float32) + head_sum(channel_terms)).astype(jnp.bfloat16)


def solution(mesh):
    return jax.shard_map(
        local,
        mesh=mesh,
        in_specs=(
            P("fs", "tp"),
            P(),
            P("fs", "tp"),
            P("fs", "tp"),
            P("fs", "tp"),
            P("fs", "tp"),
            P("tp", "fs"),
            P(),
            P("fs", "tp"),
            P("fs", "tp"),
            P(None, "tp"),
            P("tp"),
            P("tp", "fs"),
        ),
        out_specs=P("fs", "tp"),
        check_vma=False,
    )
```

profile of v0, /device:TPU:0, one launch (start us, length us, event | category | flops | bytes accessed | tf_op | source)
XLA Modules:
  0.0 415.2 jit_solution(4352974357347904392)
XLA Ops:
  7.5 10.3 %all_gather.30 = bf16[256,1536]{1,0:T(8,128)(2,1)S(1)} all-gather(bf16[256,384]{1,0:T(8,128)(2,1)} %param.15), channel_id=1, replica_groups=mesh['fs'=8,'tp'=4] {'tp'}, dimensions={1}, use_global_device_ids=true | all-gather | bytes 983040 | tf_op jit(solution)/shard_map/all_gather | solution.py:124
  18.1 32.6 %all_gather.33 = bf16[1536,192]{1,0:T(8,128)(2,1)S(1)} all-gather(bf16[192,192]{1,0:T(8,128)(2,1)S(1)} %copy-done.1), channel_id=1, replica_groups=mesh['fs'=8,'tp'=4] {'fs'}, dimensions={0}, use_global_device_ids=true | all-gather | bytes 663552 | tf_op jit(solution)/shard_map/all_gather | solution.py:15
  50.7 0.6 convolution_convert_fusion.5
  51.3 32.1 %all_gather.32 = bf16[1536,192]{1,0:T(8,128)(2,1)S(1)} all-gather(bf16[192,192]{1,0:T(8,128)(2,1)S(1)} %copy-done.2), channel_id=1, replica_groups=mesh['fs'=8,'tp'=4] {'fs'}, dimensions={0}, use_global_device_ids=true | all-gather | bytes 663552 | tf_op jit(solution)/shard_map/all_gather | solution.py:15
  83.4 0.6 convolution_convert_fusion.6
  85.7 32.2 %all_gather.31 = bf16[1536,192]{1,0:T(8,128)(2,1)S(1)} all-gather(bf16[192,192]{1,0:T(8,128)(2,1)S(1)} %copy-done.3), channel_id=1, replica_groups=mesh['fs'=8,'tp'=4] {'fs'}, dimensions={0}, use_global_device_ids=true | all-gather | bytes 663552 | tf_op jit(solution)/shard_map/all_gather | solution.py:15
  117.9 0.6 convolution_convert_fusion.7
  119.1 6.8 %while.15 = (s32[]{:T(128)}, f32[2,96,96]{2,1,0:T(8,128)S(1)}, f32[8,32,2,96]{3,1,2,0:T(8,128)S(1)}, f32[8,32,2,96]{3,1,2,0:T(8,128)S(1)}, f32[8,32,2,96]{3,2,1,...) while((s32[]{:T(128)}, f32[2,96,96]{2,1,0:T(8,128)S(1)}, ...), condition=%wide.region_2.3_spmd.clone.clone.clone, body=%wide.region_1.2_spmd.clone.clone.clone.sunk | while | flops 14241935 | bytes 455068 | solution.py:81
  119.5 0.5 convolution_add_fusion.2
  120.3 0.5 convolution_add_fusion.2
  122.0 0.5 convolution_add_fusion.2
  123.7 0.5 convolution_add_fusion.2
  124.6 0.5 convolution_add_fusion.2
  127.3 32.4 %all_gather.34 = bf16[1536,192]{1,0:T(8,128)(2,1)S(1)} all-gather(bf16[192,192]{1,0:T(8,128)(2,1)S(1)} %copy-done.4), channel_id=1, replica_groups=mesh['fs'=8,'tp'=4] {'fs'}, dimensions={0}, use_global_device_ids=true | all-gather | bytes 663552 | tf_op jit(solution)/shard_map/all_gather | solution.py:15
  159.8 31.6 %all_gather.35 = bf16[192,1536]{0,1:T(8,128)(2,1)S(1)} all-gather(bf16[192,192]{0,1:T(8,128)(2,1)S(1)} %copy.54), channel_id=1, replica_groups=mesh['fs'=8,'tp'=4] {'fs'}, dimensions={1}, use_global_device_ids=true | all-gather | bytes 663552 | tf_op jit(solution)/shard_map/all_gather | solution.py:20
  191.4 0.6 fusion.39
  192.4 1.1 copy.55
  193.6 0.5 all-gather.4.cloned.1.call-update
  194.2 0.5 all-gather.6.cloned.1.call-update
  194.8 0.5 all-gather.8.cloned.1.call-update
  195.4 21.4 %reduce-scatter.7.cloned.1.call-done = bf16[384,256]{1,0:T(8,128)(2,1)} async-done(((bf16[1536,256]{1,0:T(8,128)(2,1)}), bf16[384,256]{1,0:T(8,128)(2,1)}) %reduce-scatter.7.cloned.1.call-update) | async-done | bytes 196624
  216.8 1.1 copy.56
  217.9 7.9 %all_gather.36 = bf16[256,1536]{1,0:T(8,128)(2,1)S(1)} all-gather(bf16[256,384]{1,0:T(8,128)(2,1)S(1)} %add_convert_fusion.1), channel_id=1, replica_groups=mesh['fs'=8,'tp'=4] {'tp'}, dimensions={1}, use_global_device_ids=true | all-gather | bytes 983040 | tf_op jit(solution)/shard_map/all_gather | solution.py:124
  226.1 29.7 %all-gather.4.cloned.1.call-done = bf16[1536,1024]{1,0:T(8,128)(2,1)} async-done(((bf16[192,1024]{1,0:T(8,128)(2,1)}), bf16[1536,1024]{1,0:T(8,128)(2,1)}) %all-gather.4.cloned.1.call-update) | async-done | bytes 3145744 | tf_op jit(solution)/shard_map/all_gather | solution.py:15
  255.8 2.9 fusion.26
  258.7 57.8 %all-gather.6.cloned.1.call-done = bf16[1536,1024]{1,0:T(8,128)(2,1)} async-done(((bf16[192,1024]{1,0:T(8,128)(2,1)}), bf16[1536,1024]{1,0:T(8,128)(2,1)}) %all-gather.6.cloned.1.call-update) | async-done | bytes 3145744 | tf_op jit(solution)/shard_map/all_gather | solution.py:15
  316.5 60.7 %all-gather.8.cloned.1.call-done = bf16[1024,1536]{0,1:T(8,128)(2,1)} async-done(((bf16[1024,192]{0,1:T(8,128)(2,1)}), bf16[1024,1536]{0,1:T(8,128)(2,1)}) %all-gather.8.cloned.1.call-update) | async-done | bytes 3145744 | tf_op jit(solution)/shard_map/all_gather | solution.py:20
  377.2 5.1 %convolution_convert_fusion.1 = bf16[256,1536]{1,0:T(8,128)(2,1)S(1)} fusion(bf16[1024,1536]{0,1:T(8,128)(2,1)} %all-gather.8.cloned.1.call-done, bf16[1536,1024]{1,0:T(8,128)(2,1)} %all-gather.6.cloned.1.call-done, f32[256,1024]{1,0:T(8,128)S(1)} %fusion.26, f32[1024]{0:T(1024)S(1)} %bitcast.72, f32[1024]{0:T(1024)S(1)} %bitcast.73, ...), kind=kOutput, calls=%fused_computation.24 | convolution fusion | flops 1616248832 | bytes 8936448 | tf_op jit(solution)/shard_map/dot_general | solution.py:196
  382.3 1.2 copy.57
  383.5 22.3 %reduce-scatter.9.cloned.1.call-done = bf16[384,256]{1,0:T(8,128)(2,1)} async-done(((bf16[1536,256]{1,0:T(8,128)(2,1)}), bf16[384,256]{1,0:T(8,128)(2,1)}) %reduce-scatter.9.cloned.1.call-update) | async-done | bytes 196624
  405.8 1.1 copy.58
  406.9 0.7 add_convert_fusion
  (102 shorter events, 9.2 us)
Async XLA Ops:
  7.4 10.7 %copy-start.1 = (bf16[192,192]{1,0:T(8,128)(2,1)S(1)}, bf16[192,192]{1,0:T(8,128)(2,1)}, u32[]{:S(2)}) copy-start(bf16[192,192]{1,0:T(8,128)(2,1)} %param.18) | copy-start | bytes 221188
  7.4 43.3 %copy-start.7 = (f32[1536]{0:T(1024)S(1)}, f32[1536]{0:T(1024)}, u32[]{:S(2)}) copy-start(f32[1536]{0:T(1024)} %param.16) | copy-start | bytes 18436
  7.4 209.4 %reduce-scatter.7.cloned.1.call-start = ((), (), s32[]{:S(2)}) async-start(), calls=%async_computation.5 | async-start | bytes 983040
  18.1 33.2 %copy-start.2 = (bf16[192,192]{1,0:T(8,128)(2,1)S(1)}, bf16[192,192]{1,0:T(8,128)(2,1)}, u32[]{:S(2)}) copy-start(bf16[192,192]{1,0:T(8,128)(2,1)} %param.17) | copy-start | bytes 221188
  84.5 1.2 copy-start.3
  126.0 1.3 copy-start.4
  126.3 33.4 %copy-start.5 = (bf16[192,192]{1,0:T(8,128)(2,1)S(1)}, bf16[192,192]{1,0:T(8,128)(2,1)}, u32[]{:S(2)}) copy-start(bf16[192,192]{1,0:T(8,128)(2,1)} %param.21) | copy-start | bytes 221188
  192.4 3.0 copy-start.6
  193.5 24.3 %copy-start = (bf16[256,384]{1,0:T(8,128)(2,1)S(1)}, bf16[256,384]{1,0:T(8,128)(2,1)}, u32[]{:S(2)}) copy-start(bf16[256,384]{1,0:T(8,128)(2,1)} %param.15) | copy-start | bytes 589828
  193.6 62.2 %all-gather.4.cloned.1.call-start = ((), (), s32[]{:S(2)}) async-start(), calls=%async_computation.2 | async-start | bytes 3538944 | tf_op jit(solution)/shard_map/all_gather | solution.py:15
  194.2 122.4 %all-gather.6.cloned.1.call-start = ((), (), s32[]{:S(2)}) async-start(), calls=%async_computation.3 | async-start | bytes 3538944 | tf_op jit(solution)/shard_map/all_gather | solution.py:15
  194.7 61.1 %copy-start.8 = (f32[1536]{0:T(1024)S(1)}, f32[1536]{0:T(1024)}, u32[]{:S(2)}) copy-start(f32[1536]{0:T(1024)} %param.22) | copy-start | bytes 18436
  194.8 182.5 %all-gather.8.cloned.1.call-start = ((), (), s32[]{:S(2)}) async-start(), calls=%async_computation.4 | async-start | bytes 3538944 | tf_op jit(solution)/shard_map/all_gather | solution.py:20
  195.3 210.4 %reduce-scatter.9.cloned.1.call-start = ((), (), s32[]{:S(2)}) async-start(), calls=%async_computation.6 | async-start | bytes 983040
  226.1 151.1 %copy-start.9 = (f32[1024]{0:T(1024)S(1)}, f32[1024]{0:T(1024)}, u32[]{:S(2)}) copy-start(f32[1024]{0:T(1024)} %param.26) | copy-start | bytes 12292
Sparse Core Ops, SparseCore 0:
  193.7 23.0 reduce-scatter.6
  383.6 22.0 reduce-scatter.8
Sparse Core Ops, SparseCore 1:
  196.2 59.5 all-gather.3
  257.9 58.6 all-gather.5
  318.6 58.6 all-gather.7
where the time goes:
time: 415 us
  waiting for transfers between devices  193 us (47%)
  blocking collectives  179 us (43%)
  matrix products  17 us (4%)
  between operations  15.4 us (4%)
  local copies, waits for them, and re-layouts  6.85 us (2%)
    all_gather x4, blocking collectives, taken_in(): lax.all_gather(a, axis, axis=dim, tiled=True)  129 us
    all_gather x2, waiting for transfers between devices, taken_in(): lax.all_gather(a, axis, axis=dim, tiled=True)  87.5 us
    all_gather x1, waiting for transfers between devices, gathered_then(): whole = lax.all_gather(shard, axis, axis=dim, tiled=True)  60.7 us
    unnamed x7, waiting for transfers between devices  45.2 us
    all_gather x1, blocking collectives, gathered_then(): whole = lax.all_gather(shard, axis, axis=dim, tiled=True)  31.6 us
    all_gather x2, blocking collectives, features(): return lax.all_gather(shard, 'tp', axis=1, tiled=True)  18.3 us
  transfers between devices with their start and end apart: 5, of which 5 were waited for; matrix products, arithmetic and copies ran while one was open for 1% of the time, Pallas kernels for 0%

commit v1 on v0

--- a/solution.py
+++ b/solution.py
@@ -1,6 +1,9 @@
 import jax
 import jax.numpy as jnp
+import numpy as np
 from jax import lax
+from jax.experimental import pallas as pl
+from jax.experimental.pallas import tpu as pltpu
 from jax.sharding import PartitionSpec as P
 
 BLOCK = 32
@@ -199,9 +202,447 @@
     return (middle.astype(jnp.float32) + head_sum(channel_terms)).astype(jnp.bfloat16)
 
 
+LANES = 128
+MESH = pl.DeviceIdType.MESH
+
+
+def padded_lanes(piece):
+    return jnp.pad(piece, ((0, 0), (0, LANES - piece.shape[1])))
+
+
+def dot(left, right):
+    return jnp.dot(left, right, preferred_element_type=jnp.float32)
+
+
+def dot_t(left, right):
+    return lax.dot_general(left, right, (((1,), (1,)), ((), ())), preferred_element_type=jnp.float32)
+
+
+def layer_kernel(
+    fs_count,
+    heads,
+    tokens_ref,
+    gain_in_ref,
+    gain_mid_ref,
+    wa_ref,
+    wg_ref,
+    wv_ref,
+    wd_ref,
+    taps_ref,
+    bias_ref,
+    cos_ref,
+    sin_ref,
+    turn_ref,
+    out_ref,
+    ga,
+    gg,
+    gv,
+    gd,
+    tok_all,
+    mid_all,
+    part_mix,
+    part_ch,
+    land_mix,
+    land_ch,
+    normed,
+    w_send,
+    w_recv,
+    w_own,
+    ag_send,
+    ag_recv,
+    ag_own,
+    rs_send,
+    rs_recv,
+    hidden_gate,
+    hidden,
+    middle,
+):
+    fs = lax.axis_index("fs")
+    tp = lax.axis_index("tp")
+    z, x = fs // 2, fs % 2
+    y, c = tp // 2, tp % 2
+    zl = z % 2
+    z_count = fs_count // 2
+    rows, width = tokens_ref.shape
+    depth = wa_ref.shape[1]
+    tp_count = 4
+    z_mate = (z + 1 - 2 * zl) * 2 + x
+    x_mate = z * 2 + 1 - x
+    y_mate = (1 - y) * 2 + c
+    c_mate = y * 2 + 1 - c
+    to_z, to_x, to_y, to_c = (z_mate, tp), (x_mate, tp), (fs, y_mate), (fs, c_mate)
+    z_peers = [lax.rem(z + step, z_count) for step in range(1, z_count)]
+
+    barrier = pltpu.get_barrier_semaphore()
+    greeted = [(zp * 2 + x, tp) for zp in z_peers] + [to_x, to_y, to_c]
+    for peer in greeted:
+        pl.semaphore_signal(barrier, inc=1, device_id=peer, device_id_type=MESH)
+    pl.semaphore_wait(barrier, len(greeted))
+
+    sends = []
+
+    def remote(src, dst, send_sem, recv_sem, peer):
+        copy = pltpu.make_async_remote_copy(
+            src_ref=src,
+            dst_ref=dst,
+            send_sem=send_sem,
+            recv_sem=recv_sem,
+            device_id=peer,
+            device_id_type=MESH,
+        )
+        copy.start()
+        sends.append(copy)
+
+    def arrived(ref, sem):
+        pltpu.make_async_remote_copy(
+            src_ref=ref,
+            dst_ref=ref,
+            send_sem=sem,
+            recv_sem=sem,
+            device_id=to_c,
+            device_id_type=MESH,
+        ).wait_recv()
+
+    def slot(held, owner):
+        return held.at[pl.ds(pl.multiple_of(owner * depth, depth), depth)]
+
+    chunks = [(wa_ref, ga), (wg_ref, gg), (wv_ref, gv), (wd_ref, gd)]
+    own_copies = []
+
+    def weights_out(k):
+        shard, held = chunks[k]
+        for i, zp in enumerate(z_peers):
+            remote(
+                shard.at[zp % 2],
+                slot(held, fs),
+                w_send.at[k, i],
+                w_recv.at[k, fs],
+                (zp * 2 + x, tp),
+            )
+        remote(
+            shard.at[zl], slot(held, fs), w_send.at[k, z_count - 1], w_recv.at[k, fs], to_x
+        )
+        own = pltpu.make_async_copy(shard.at[zl], slot(held, fs), w_own.at[k])
+        own.start()
+        own_copies.append(own)
+
+    def weights_on(k):
+        held = chunks[k][1]
+        for i in range(z_count - 1):
+            owner = lax.rem(z + z_count - 1 - i, z_count) * 2 + x
+            arrived(slot(held, owner), w_recv.at[k, owner])
+            remote(
+                slot(held, owner),
+                slot(held, owner),
+                w_send.at[k, z_count + i],
+                w_recv.at[k, owner],
+                to_x,
+            )
+
+    def weights_in(k):
+        held = chunks[k][1]
+        own_copies[k].wait()
+        for step in range(z_count):
+            owner = lax.rem(z + z_count - step, z_count) * 2 + 1 - x
+            arrived(slot(held, owner), w_recv.at[k, owner])
+
+    mine = zl * 4 + tp
+    from_z = (1 - zl) * 4 + tp
+    from_y = zl * 4 + y_mate
+    from_zy = (1 - zl) * 4 + y_mate
+    gathered = (mine, from_z, from_y, from_zy)
+
+    def gather_start(phase, src, held):
+        def pass_on(which, ref, block, peer):
+            remote(
+                ref, held.at[block], ag_send.at[phase, which], ag_recv.at[phase, block], peer
+            )
+
+        pass_on(0, src, mine, to_z)
+        pass_on(1, src, mine, to_y)
+        pass_on(2, src, mine, to_c)
+        own = pltpu.make_async_copy(src, held.at[mine], ag_own.at[phase])
+        own.start()
+        return pass_on, own
+
+    def gather_end(phase, held, state):
+        pass_on, own = state
+        arrived(held.at[from_z], ag_recv.at[phase, from_z])
+        pass_on(3, held.at[from_z], from_z, to_y)
+        pass_on(4, held.at[from_z], from_z, to_c)
+        arrived(held.at[from_y], ag_recv.at[phase, from_y])
+        pass_on(5, held.at[from_y], from_y, to_c)
+        arrived(held.at[from_zy], ag_recv.at[phase, from_zy])
+        pass_on(6, held.at[from_zy], from_zy, to_c)
+        own.wait()
+        for half in range(2):
+            for side in range(2):
+                block = half * 4 + side * 2 + 1 - c
+                arrived(held.at[block], ag_recv.at[phase, block])
+
+    def add_into(parts, block, land, where):
+        parts[block] = (
+            parts[block].astype(jnp.float32) + land[where].astype(jnp.float32)
+        ).astype(jnp.bfloat16)
+
+    def scatter(phase, parts, land, between):
+        def give(which, block, peer):
+            remote(
+                parts.at[block],
+                land.at[which],
+                rs_send.at[phase, which],
+                rs_recv.at[phase, which],
+                peer,
+            )
+
+        def take(which):
+            arrived(land.at[which], rs_recv.at[phase, which])
+
+        for side in (1 - y, y):
+            for half in (1 - zl, zl):
+                give(half * 2 + side, half * 4 + side * 2 + 1 - c, to_c)
+        for half in (1 - zl, zl):
+            which = half * 2 + 1 - y
+            take(which)
+            block = half * 4 + (1 - y) * 2 + c
+            add_into(parts, block, land, which)
+            give(4 + half, block, to_y)
+        between()
+        for half in (1 - zl, zl):
+            which = half * 2 + y
+            take(which)
+            add_into(parts, half * 4 + tp, land, which)
+        take(4 + 1 - zl)
+        add_into(parts, from_z, land, 4 + 1 - zl)
+        give(6, from_z, to_z)
+        take(4 + zl)
+        total = parts[mine].astype(jnp.float32) + land[4 + zl].astype(jnp.float32)
+        take(6)
+        return total + land[6].astype(jnp.float32)
+
+    def normalise(held, gain_ref):
+        @pl.loop(0, 2)
+        def _(half):
+            squares = jnp.zeros((rows, 1), jnp.float32)
+            for t in range(tp_count):
+                wide = held[half * 4 + t].astype(jnp.float32)
+                squares = squares + jnp.sum(wide * wide, axis=-1, keepdims=True)
+            scale = lax.rsqrt(squares / (tp_count * width) + epsilon)
+            for t in range(tp_count):
+                wide = held[half * 4 + t].astype(jnp.float32)
+                normed[half * 4 + t] = (
+                    wide * scale * gain_ref[:, t * width : (t + 1) * width]
+                ).astype(jnp.bfloat16)
+
+    def project(half, held, columns):
+        total = dot(normed[half * 4], held[0:width, 0:columns])
+        for t in range(1, tp_count):
+            total = total + dot(
+                normed[half * 4 + t], held[t * width : (t + 1) * width, 0:columns]
+            )
+        return total.astype(jnp.bfloat16)
+
+    state = gather_start(0, tokens_ref, tok_all)
+    weights_out(0)
+    weights_out(1)
+    gather_end(0, tok_all, state)
+    normalise(tok_all, gain_in_ref)
+    weights_on(0)
+    weights_out(2)
+    weights_in(0)
+
+    head = tp * 2 + zl
+    log_gamma = jnp.float32(0.0)
+    for j in range(heads):
+        log_gamma = jnp.where(head == j, jnp.float32(np.log1p(-(2.0 ** (-5.0 - j)))), log_gamma)
+
+    @pl.loop(0, 2)
+    def _(half):
+        wide = project(half, ga, 4 * LANES)
+        turn = turn_ref[...]
+
+        def rotated(piece):
+            return piece.astype(jnp.float32) * cos_ref[...] + dot(piece, turn) * sin_ref[...]
+
+        query_r = rotated(wide[:, 0:LANES]).astype(jnp.bfloat16)
+        key_r = (rotated(wide[:, LANES : 2 * LANES]) * HEAD_DIM ** (-0.5)).astype(jnp.bfloat16)
+        value = wide[:, 2 * LANES : 3 * LANES]
+        gate = wide[:, 3 * LANES : 4 * LANES].astype(jnp.float32)
+        later = lax.broadcasted_iota(jnp.int32, (rows, rows), 0)
+        earlier = lax.broadcasted_iota(jnp.int32, (rows, rows), 1)
+        lag = later - earlier
+        decay = jnp.where(
+            lag >= 0, jnp.exp(log_gamma * jnp.maximum(lag, 0).astype(jnp.float32)), 0.0
+        )
+        scores = dot_t(query_r, key_r) * decay
+        coarse = scores.astype(jnp.bfloat16)
+        fine = (scores - coarse.astype(jnp.float32)).astype(jnp.bfloat16)
+        retained = dot(coarse, value) + dot(fine, value)
+        square = jnp.sum(retained * retained, axis=-1, keepdims=True) / HEAD_DIM
+        gated = (
+            retained * lax.rsqrt(square + epsilon) * (gate * (1.0 / (1.0 + jnp.exp(-gate))))
+        ).astype(jnp.bfloat16)
+        for t in range(tp_count):
+            part_mix[half * 4 + t] = dot_t(
+                gated, ga[t * width : (t + 1) * width, 4 * LANES : 5 * LANES]
+            ).astype(jnp.bfloat16)
+
+    mixed = scatter(0, part_mix, land_mix, lambda: weights_on(1))
+    middle[...] = (tokens_ref[...].astype(jnp.float32) + mixed).astype(jnp.bfloat16)
+    state = gather_start(1, middle, mid_all)
+    weights_out(3)
+    gather_end(1, mid_all, state)
+    weights_on(2)
+    normalise(mid_all, gain_mid_ref)
+    weights_in(1)
+
+    @pl.loop(0, 2)
+    def _(half):
+        up = project(half, gg, gg.shape[1]).astype(jnp.float32)
+        at = lax.broadcasted_iota(jnp.int32, up.shape, 0)
+        taps = taps_ref[zl]
+        tap_count = taps.shape[0]
+        summed = up * taps[tap_count - 1 : tap_count] + bias_ref[zl]
+        for back in range(1, tap_count):
+            moved = jnp.where(at >= back, pltpu.roll(up, back, 0), 0.0)
+            summed = summed + moved * taps[tap_count - 1 - back : tap_count - back]
+        hidden_gate[half] = summed * (1.0 / (1.0 + jnp.exp(-summed)))
+
+    weights_on(3)
+    weights_in(2)
+
+    @pl.loop(0, 2)
+    def _(half):
+        value_up = project(half, gv, gv.shape[1]).astype(jnp.float32)
+        hidden[half] = (hidden_gate[half] * value_up).astype(jnp.bfloat16)
+
+    weights_in(3)
+
+    @pl.loop(0, 2)
+    def _(half):
+        for t in range(tp_count):
+            part_ch[half * 4 + t] = dot_t(
+                hidden[half], gd[t * width : (t + 1) * width]
+            ).astype(jnp.bfloat16)
+
+    summed = scatter(1, part_ch, land_ch, lambda: None)
+    result = (middle[...].astype(jnp.float32) + summed).astype(jnp.bfloat16)
+    for copy in sends:
+        copy.wait_send()
+    out_ref[...] = result
+
+
+def rotation_tables(length):
+    half_width = HEAD_DIM // 2
+    inv_freq = rotary_base ** (-np.arange(half_width) / half_width)
+    angles = np.arange(length)[:, None] * inv_freq[None, :]
+    angles = np.pad(np.concatenate([angles, angles], axis=1), ((0, 0), (0, LANES - HEAD_DIM)))
+    turn = np.zeros((LANES, LANES), np.float32)
+    for i in range(half_width):
+        turn[i + half_width, i] = -1.0
+        turn[i, i + half_width] = 1.0
+    return np.cos(angles).astype(np.float32), np.sin(angles).astype(np.float32), turn
+
+
+def fused(
+    fs_count,
+    heads,
+    tokens,
+    norm_in_gain,
+    query_w,
+    key_w,
+    value_w,
+    gate_w,
+    out_w,
+    norm_mid_gain,
+    up_gate_w,
+    up_value_w,
+    conv_taps,
+    conv_bias,
+    down_w,
+):
+    rows, width = tokens.shape
+    hidden_half = up_gate_w.shape[1] // 2
+
+    def of_half(b):
+        head = slice(b * HEAD_DIM, (b + 1) * HEAD_DIM)
+        pieces = [padded_lanes(w[:, head]) for w in (query_w, key_w, value_w, gate_w)]
+        return jnp.concatenate(pieces + [padded_lanes(out_w[head].T)], axis=1)
+
+    wa = jnp.stack([of_half(0), of_half(1)])
+    wg = jnp.stack([up_gate_w[:, :hidden_half], up_gate_w[:, hidden_half:]])
+    wv = jnp.stack([up_value_w[:, :hidden_half], up_value_w[:, hidden_half:]])
+    wd = jnp.stack([down_w[:hidden_half].T, down_w[hidden_half:].T])
+    taps = jnp.stack([conv_taps[:, :hidden_half], conv_taps[:, hidden_half:]])
+    bias = conv_bias.reshape(2, 1, hidden_half)
+    cosine, sine, turn = rotation_tables(rows)
+    features_all = wa.shape[1] * fs_count
+    block = (rows, width)
+
+    def held(shard):
+        return pltpu.VMEM((features_all, shard.shape[2]), jnp.bfloat16)
+
+    z_count = fs_count // 2
+    return pl.pallas_call(
+        lambda *refs: layer_kernel(fs_count, heads, *refs),
+        out_shape=jax.ShapeDtypeStruct(block, jnp.bfloat16),
+        in_specs=[pl.BlockSpec(memory_space=pltpu.VMEM)] * 12,
+        out_specs=pl.BlockSpec(memory_space=pltpu.VMEM),
+        scratch_shapes=[
+            held(wa),
+            held(wg),
+            held(wv),
+            held(wd),
+            pltpu.VMEM((8,) + block, jnp.bfloat16),
+            pltpu.VMEM((8,) + block, jnp.bfloat16),
+            pltpu.VMEM((8,) + block, jnp.bfloat16),
+            pltpu.VMEM((8,) + block, jnp.bfloat16),
+            pltpu.VMEM((7,) + block, jnp.bfloat16),
+            pltpu.VMEM((7,) + block, jnp.bfloat16),
+            pltpu.VMEM((8,) + block, jnp.bfloat16),
+            pltpu.SemaphoreType.DMA((4, 2 * z_count - 1)),
+            pltpu.SemaphoreType.DMA((4, fs_count)),
+            pltpu.SemaphoreType.DMA((4,)),
+            pltpu.SemaphoreType.DMA((2, 7)),
+            pltpu.SemaphoreType.DMA((2, 8)),
+            pltpu.SemaphoreType.DMA((2,)),
+            pltpu.SemaphoreType.DMA((2, 7)),
+            pltpu.SemaphoreType.DMA((2, 7)),
+            pltpu.VMEM((2, rows, hidden_half), jnp.float32),
+            pltpu.VMEM((2, rows, hidden_half), jnp.bfloat16),
+            pltpu.VMEM(block, jnp.bfloat16),
+        ],
+        compiler_params=pltpu.CompilerParams(
+            collective_id=0, has_side_effects=True, vmem_limit_bytes=60 * 1024 * 1024
+        ),
+        name="layer",
+    )(
+        tokens,
+        norm_in_gain.reshape(1, -1),
+        norm_mid_gain.reshape(1, -1),
+        wa,
+        wg,
+        wv,
+        wd,
+        taps,
+        bias,
+        jnp.asarray(cosine),
+        jnp.asarray(sine),
+        jnp.asarray(turn, jnp.bfloat16),
+    )
+
+
 def solution(mesh):
+    fs_count, tp_count = mesh.shape["fs"], mesh.shape["tp"]
+
+    def step(*args):
+        local_heads = args[2].shape[1] // HEAD_DIM
+        if local_heads == 2 and tp_count == 4 and fs_count == 8:
+            return fused(fs_count, local_heads * tp_count, *args)
+        return local(*args)
+
     return jax.shard_map(
-        local,
+        step,
         mesh=mesh,
         in_specs=(
             P("fs", "tp"),

time: 415 us -> 135 us (0.33)
  waiting for transfers between devices: 193 us -> 0 us
  blocking collectives: 179 us -> 0 us
  Pallas kernels: 0 us -> 123 us
  matrix products: 17 us -> 0 us
  between operations: 15.4 us -> 0.15 us
    all_gather x7 -> x0, blocking collectives: 179 us -> none  [the longest x4 129 us: taken_in(): lax.all_gather(a, axis, axis=dim, tiled=True)]
    all_gather x3 -> x0, waiting for transfers between devices: 148 us -> none  [the longest x2 87.5 us: taken_in(): lax.all_gather(a, axis, axis=dim, tiled=True)]
    pallas_call x0 -> x1, Pallas kernels: none -> 123 us  [fused(): pl.pallas_call(lambda *refs: layer_kernel(fs_count, heads, *refs), out_sh...]
    unnamed x7 -> x0, waiting for transfers between devices: 45.2 us -> none
    dot_general x25 -> x0, matrix products: 17 us -> none  [the longest x5 5.15 us: add_single(): jnp.dot(columns, weight_piece, preferred_element_type=jnp.float32)]
  transfers between devices with their start and end apart: 5 -> 0, of which waited for: 5 -> 0; matrix products, arithmetic and copies ran while one was open for 1% -> 0% of each run, Pallas kernels for 0% -> 0%
where the time goes in v1:
time: 135 us
  Pallas kernels  123 us (91%)
  local copies, waits for them, and re-layouts  8.96 us (7%)
  other arithmetic  3.27 us (2%)
    pallas_call x1, Pallas kernels, fused(): pl.pallas_call(lambda *refs: layer_kernel(fs_count, heads, *refs), out_sh...  123 us
    unnamed x29, local copies, waits for them, and re-layouts  6.21 us

profile of v1, /device:TPU:0, one launch (start us, length us, event | category | flops | bytes accessed | tf_op | source)
XLA Modules:
  0.0 134.9 jit_solution(505418605108363658)
XLA Ops:
  0.0 0.0 copy-start
  0.0 1.1 slice_bitcast_fusion.5
  1.1 0.1 copy-done
  1.2 0.0 copy-start.2
  1.2 1.0 pad_maximum_fusion.1
  2.2 0.0 copy-done.2
  2.2 0.0 copy-start.3
  2.2 0.1 copy.20
  2.3 0.8 copy-done.3
  3.1 0.1 slice.63
  3.2 0.8 copy-done.4
  4.0 0.1 slice.64
  4.1 0.8 copy-done.5
  4.9 0.1 slice.65
  5.0 0.8 copy-done.6
  5.8 0.1 slice.66
  5.9 0.1 copy.19
  6.0 0.0 copy-start.8
  6.0 0.7 copy-done.8
  6.8 0.0 copy-start.1
  6.8 0.8 pad_maximum_fusion.refs_3_
  7.7 0.2 copy-done.1
  8.0 0.0 copy-start.7
  8.0 0.8 pad_maximum_fusion.3.refs_6_
  8.8 0.0 copy-done.7
  8.8 0.6 pad_maximum_fusion.4.refs_7_
  9.4 0.1 copy-done.9
  9.5 0.6 reshape.10.refs_2_
  10.1 0.1 copy-done.10
  10.2 0.6 reshape.9.refs_1_
  10.8 122.5 %layer.1 = bf16[256,384]{1,0:T(8,128)(2,1)} custom-call(bf16[256,384]{1,0:T(8,128)(2,1)} %refs_0_.1, f32[1,1536]{1,0:T(1,128)} %reshape.9.refs_1_, f32[1,1536]{1,0:T(1,128)} %reshape.10.refs_2_, bf16[2,192,640]{2,1,0:T(8,128)(2,1)} %pad_maximum_fusion.refs_3_, bf16[2,192,512]{2,1,0:T(8,128)(2,1)} %get-tuple-element.15.refs_4_, ...), custom_call_target="tpu_custom_call" | custom-call | tf_op jit(solution)/shard_map/layer/pallas_call | solution.py:586
  133.3 1.6 %copy.30 = bf16[256,384]{1,0:T(8,128)(2,1)} copy(bf16[256,384]{1,0:T(8,128)(2,1)} %layer.1) | data formatting | bytes 393216
  (19 shorter events, 0.3 us)
Async XLA Ops:
  0.0 1.2 copy-start
  1.2 1.0 copy-start.2
  2.2 0.9 copy-start.3
  3.1 0.9 copy-start.4
  4.0 0.9 copy-start.5
  4.9 0.9 copy-start.6
  6.0 0.7 copy-start.8
  6.8 1.1 copy-start.1
  8.0 0.8 copy-start.7
  8.8 0.7 copy-start.9
  9.5 0.7 copy-start.10

commit v2 on v1

--- a/solution.py
+++ b/solution.py
@@ -206,10 +206,6 @@
 MESH = pl.DeviceIdType.MESH
 
 
-def padded_lanes(piece):
-    return jnp.pad(piece, ((0, 0), (0, LANES - piece.shape[1])))
-
-
 def dot(left, right):
     return jnp.dot(left, right, preferred_element_type=jnp.float32)
 
@@ -221,19 +217,22 @@
 def layer_kernel(
     fs_count,
     heads,
-    tokens_ref,
-    gain_in_ref,
-    gain_mid_ref,
+    *refs,
+):
+    count = 16
+    sources, out_ref, local_refs, load_sem = refs[:count], refs[count], refs[count + 1 : 2 * count + 1], refs[2 * count + 1]
+    layer_body(fs_count, heads, sources, local_refs, load_sem, out_ref, *refs[2 * count + 2 :])
+
+
+def layer_body(
+    fs_count,
+    heads,
+    sources,
+    local_refs,
+    load_sem,
+    out_ref,
     wa_ref,
-    wg_ref,
-    wv_ref,
     wd_ref,
-    taps_ref,
-    bias_ref,
-    cos_ref,
-    sin_ref,
-    turn_ref,
-    out_ref,
     ga,
     gg,
     gv,
@@ -256,7 +255,32 @@
     hidden_gate,
     hidden,
     middle,
+    land_half,
 ):
+    loads = [
+        pltpu.make_async_copy(source, here, load_sem.at[i])
+        for i, (source, here) in enumerate(zip(sources, local_refs))
+    ]
+    for load in loads:
+        load.start()
+    (
+        tokens_ref,
+        query_ref,
+        key_ref,
+        value_ref,
+        gate_ref,
+        o_ref,
+        wg_ref,
+        wv_ref,
+        down_ref,
+        gain_in_ref,
+        gain_mid_ref,
+        taps_ref,
+        bias_ref,
+        cos_ref,
+        sin_ref,
+        turn_ref,
+    ) = local_refs
     fs = lax.axis_index("fs")
     tp = lax.axis_index("tp")
     z, x = fs // 2, fs % 2
@@ -277,6 +301,17 @@
     greeted = [(zp * 2 + x, tp) for zp in z_peers] + [to_x, to_y, to_c]
     for peer in greeted:
         pl.semaphore_signal(barrier, inc=1, device_id=peer, device_id_type=MESH)
+    for load in loads[:6]:
+        load.wait()
+    hidden_half = wd_ref.shape[2]
+    for b in range(2):
+        head_rows = slice(b * HEAD_DIM, (b + 1) * HEAD_DIM)
+        pieces = [w[...][:, head_rows] for w in (query_ref, key_ref, value_ref, gate_ref)]
+        pieces.append(o_ref[head_rows].T)
+        pieces.append(jnp.zeros((o_ref.shape[1], wa_ref.shape[2] - 5 * HEAD_DIM), jnp.bfloat16))
+        wa_ref[b] = jnp.concatenate(pieces, axis=1)
+    for load in loads[6:]:
+        load.wait()
     pl.semaphore_wait(barrier, len(greeted))
 
     sends = []
@@ -311,18 +346,25 @@
 
     def weights_out(k):
         shard, held = chunks[k]
+
+        def part(b):
+            if k in (1, 2):
+                start = pl.multiple_of(b * hidden_half, LANES)
+                return shard.at[:, pl.ds(start, hidden_half)]
+            return shard.at[b]
+
         for i, zp in enumerate(z_peers):
             remote(
-                shard.at[zp % 2],
+                part(zp % 2),
                 slot(held, fs),
                 w_send.at[k, i],
                 w_recv.at[k, fs],
                 (zp * 2 + x, tp),
             )
         remote(
-            shard.at[zl], slot(held, fs), w_send.at[k, z_count - 1], w_recv.at[k, fs], to_x
+            part(zl), slot(held, fs), w_send.at[k, z_count - 1], w_recv.at[k, fs], to_x
         )
-        own = pltpu.make_async_copy(shard.at[zl], slot(held, fs), w_own.at[k])
+        own = pltpu.make_async_copy(part(zl), slot(held, fs), w_own.at[k])
         own.start()
         own_copies.append(own)
 
@@ -385,7 +427,7 @@
             parts[block].astype(jnp.float32) + land[where].astype(jnp.float32)
         ).astype(jnp.bfloat16)
 
-    def scatter(phase, parts, land, between):
+    def scatter(phase, parts, land, between, waiting):
         def give(which, block, peer):
             remote(
                 parts.at[block],
@@ -415,10 +457,58 @@
         take(4 + 1 - zl)
         add_into(parts, from_z, land, 4 + 1 - zl)
         give(6, from_z, to_z)
+        waiting()
         take(4 + zl)
         total = parts[mine].astype(jnp.float32) + land[4 + zl].astype(jnp.float32)
         take(6)
         return total + land[6].astype(jnp.float32)
+
+    def scatter_out(parts, land):
+        top, low = pl.ds(0, rows // 2), pl.ds(rows // 2, rows // 2)
+
+        def give(which, src, dst, peer):
+            remote(src, dst, rs_send.at[1, which], rs_recv.at[1, which], peer)
+
+        def give_half(which, block, part, peer):
+            give(4 + which, parts.at[block, part], land_half.at[which], peer)
+
+        def take(which, ref):
+            arrived(ref, rs_recv.at[1, which])
+
+        def take_half(which):
+            take(4 + which, land_half.at[which])
+            return land_half[which].astype(jnp.float32)
+
+        for half, side in ((1 - zl, 1 - y), (zl, 1 - y), (1 - zl, y), (zl, y)):
+            which = half * 2 + side
+            give(which, parts.at[half * 4 + side * 2 + 1 - c], land.at[which], to_c)
+
+        def settle(half, side):
+            which = half * 2 + side
+            take(which, land.at[which])
+            add_into(parts, half * 4 + side * 2 + c, land, which)
+
+        settle(1 - zl, 1 - y)
+        give_half(0, from_zy, top, to_y)
+        give_half(3, from_zy, low, to_z)
+        settle(zl, 1 - y)
+        give_half(1, from_y, top, to_y)
+        settle(1 - zl, y)
+        give_half(4, from_z, low, to_z)
+        settle(zl, y)
+        parts[from_z, top] = (parts[from_z, top].astype(jnp.float32) + take_half(0)).astype(
+            jnp.bfloat16
+        )
+        give_half(2, from_z, top, to_z)
+        parts[from_y, low] = (parts[from_y, low].astype(jnp.float32) + take_half(3)).astype(
+            jnp.bfloat16
+        )
+        give_half(5, from_y, low, to_y)
+        base = middle[...].astype(jnp.float32) + parts[mine].astype(jnp.float32)
+        upper = base[: rows // 2] + take_half(1)
+        lower = base[rows // 2 :] + take_half(4)
+        out_ref[top] = (upper + take_half(2)).astype(jnp.bfloat16)
+        out_ref[low] = (lower + take_half(5)).astype(jnp.bfloat16)
 
     def normalise(held, gain_ref):
         @pl.loop(0, 2)
@@ -431,7 +521,7 @@
             for t in range(tp_count):
                 wide = held[half * 4 + t].astype(jnp.float32)
                 normed[half * 4 + t] = (
-                    wide * scale * gain_ref[:, t * width : (t + 1) * width]
+                    wide * scale * gain_ref[t * width : (t + 1) * width][None, :]
                 ).astype(jnp.bfloat16)
 
     def project(half, held, columns):
@@ -445,10 +535,13 @@
     state = gather_start(0, tokens_ref, tok_all)
     weights_out(0)
     weights_out(1)
+    weights_out(2)
+    for b in range(2):
+        wd_ref[b] = down_ref[b * hidden_half : (b + 1) * hidden_half].T
+    weights_out(3)
     gather_end(0, tok_all, state)
     normalise(tok_all, gain_in_ref)
     weights_on(0)
-    weights_out(2)
     weights_in(0)
 
     head = tp * 2 + zl
@@ -458,16 +551,16 @@
 
     @pl.loop(0, 2)
     def _(half):
-        wide = project(half, ga, 4 * LANES)
+        wide = project(half, ga, ga.shape[1])
         turn = turn_ref[...]
 
         def rotated(piece):
             return piece.astype(jnp.float32) * cos_ref[...] + dot(piece, turn) * sin_ref[...]
 
-        query_r = rotated(wide[:, 0:LANES]).astype(jnp.bfloat16)
-        key_r = (rotated(wide[:, LANES : 2 * LANES]) * HEAD_DIM ** (-0.5)).astype(jnp.bfloat16)
-        value = wide[:, 2 * LANES : 3 * LANES]
-        gate = wide[:, 3 * LANES : 4 * LANES].astype(jnp.float32)
+        query_r = rotated(wide[:, 0 * HEAD_DIM : 1 * HEAD_DIM]).astype(jnp.bfloat16)
+        key_r = (rotated(wide[:, 1 * HEAD_DIM : 2 * HEAD_DIM]) * HEAD_DIM ** (-0.5)).astype(jnp.bfloat16)
+        value = wide[:, 2 * HEAD_DIM : 3 * HEAD_DIM]
+        gate = wide[:, 3 * HEAD_DIM : 4 * HEAD_DIM].astype(jnp.float32)
         later = lax.broadcasted_iota(jnp.int32, (rows, rows), 0)
         earlier = lax.broadcasted_iota(jnp.int32, (rows, rows), 1)
         lag = later - earlier
@@ -484,15 +577,14 @@
         ).astype(jnp.bfloat16)
         for t in range(tp_count):
             part_mix[half * 4 + t] = dot_t(
-                gated, ga[t * width : (t + 1) * width, 4 * LANES : 5 * LANES]
+                gated, ga[t * width : (t + 1) * width, 4 * HEAD_DIM : 5 * HEAD_DIM]
             ).astype(jnp.bfloat16)
 
-    mixed = scatter(0, part_mix, land_mix, lambda: weights_on(1))
+    mixed = scatter(0, part_mix, land_mix, lambda: (weights_on(1)), lambda: (weights_on(2)))
     middle[...] = (tokens_ref[...].astype(jnp.float32) + mixed).astype(jnp.bfloat16)
     state = gather_start(1, middle, mid_all)
-    weights_out(3)
+    weights_on(3)
     gather_end(1, mid_all, state)
-    weights_on(2)
     normalise(mid_all, gain_mid_ref)
     weights_in(1)
 
@@ -500,15 +592,14 @@
     def _(half):
         up = project(half, gg, gg.shape[1]).astype(jnp.float32)
         at = lax.broadcasted_iota(jnp.int32, up.shape, 0)
-        taps = taps_ref[zl]
+        taps = taps_ref[:, pl.ds(pl.multiple_of(zl * hidden_half, LANES), hidden_half)]
         tap_count = taps.shape[0]
-        summed = up * taps[tap_count - 1 : tap_count] + bias_ref[zl]
+        summed = up * taps[tap_count - 1 : tap_count] + bias_ref[pl.ds(pl.multiple_of(zl * hidden_half, LANES), hidden_half)][None, :]
         for back in range(1, tap_count):
             moved = jnp.where(at >= back, pltpu.roll(up, back, 0), 0.0)
             summed = summed + moved * taps[tap_count - 1 - back : tap_count - back]
         hidden_gate[half] = summed * (1.0 / (1.0 + jnp.exp(-summed)))
 
-    weights_on(3)
     weights_in(2)
 
     @pl.loop(0, 2)
@@ -525,19 +616,17 @@
                 hidden[half], gd[t * width : (t + 1) * width]
             ).astype(jnp.bfloat16)
 
-    summed = scatter(1, part_ch, land_ch, lambda: None)
-    result = (middle[...].astype(jnp.float32) + summed).astype(jnp.bfloat16)
+    scatter_out(part_ch, land_ch)
     for copy in sends:
         copy.wait_send()
-    out_ref[...] = result
 
 
 def rotation_tables(length):
     half_width = HEAD_DIM // 2
     inv_freq = rotary_base ** (-np.arange(half_width) / half_width)
     angles = np.arange(length)[:, None] * inv_freq[None, :]
-    angles = np.pad(np.concatenate([angles, angles], axis=1), ((0, 0), (0, LANES - HEAD_DIM)))
-    turn = np.zeros((LANES, LANES), np.float32)
+    angles = np.concatenate([angles, angles], axis=1)
+    turn = np.zeros((HEAD_DIM, HEAD_DIM), np.float32)
     for i in range(half_width):
         turn[i + half_width, i] = -1.0
         turn[i, i + half_width] = 1.0
@@ -564,35 +653,49 @@
     rows, width = tokens.shape
     hidden_half = up_gate_w.shape[1] // 2
 
-    def of_half(b):
-        head = slice(b * HEAD_DIM, (b + 1) * HEAD_DIM)
-        pieces = [padded_lanes(w[:, head]) for w in (query_w, key_w, value_w, gate_w)]
-        return jnp.concatenate(pieces + [padded_lanes(out_w[head].T)], axis=1)
-
-    wa = jnp.stack([of_half(0), of_half(1)])
-    wg = jnp.stack([up_gate_w[:, :hidden_half], up_gate_w[:, hidden_half:]])
-    wv = jnp.stack([up_value_w[:, :hidden_half], up_value_w[:, hidden_half:]])
-    wd = jnp.stack([down_w[:hidden_half].T, down_w[hidden_half:].T])
-    taps = jnp.stack([conv_taps[:, :hidden_half], conv_taps[:, hidden_half:]])
-    bias = conv_bias.reshape(2, 1, hidden_half)
     cosine, sine, turn = rotation_tables(rows)
-    features_all = wa.shape[1] * fs_count
+    depth = query_w.shape[0]
+    features_all = depth * fs_count
+    first = -(-5 * HEAD_DIM // LANES) * LANES
     block = (rows, width)
 
-    def held(shard):
-        return pltpu.VMEM((features_all, shard.shape[2]), jnp.bfloat16)
+    def held(columns):
+        return pltpu.VMEM((features_all, columns), jnp.bfloat16)
+
+    operands = (
+        tokens,
+        query_w,
+        key_w,
+        value_w,
+        gate_w,
+        out_w,
+        up_gate_w,
+        up_value_w,
+        down_w,
+        norm_in_gain,
+        norm_mid_gain,
+        conv_taps,
+        conv_bias,
+        jnp.asarray(cosine),
+        jnp.asarray(sine),
+        jnp.asarray(turn, jnp.bfloat16),
+    )
 
     z_count = fs_count // 2
     return pl.pallas_call(
         lambda *refs: layer_kernel(fs_count, heads, *refs),
         out_shape=jax.ShapeDtypeStruct(block, jnp.bfloat16),
-        in_specs=[pl.BlockSpec(memory_space=pltpu.VMEM)] * 12,
+        in_specs=[pl.BlockSpec(memory_space=pl.ANY)] * len(operands),
         out_specs=pl.BlockSpec(memory_space=pltpu.VMEM),
         scratch_shapes=[
-            held(wa),
-            held(wg),
-            held(wv),
-            held(wd),
+            *[pltpu.VMEM(array.shape, array.dtype) for array in operands],
+            pltpu.SemaphoreType.DMA((len(operands),)),
+            pltpu.VMEM((2, depth, first), jnp.bfloat16),
+            pltpu.VMEM((2, depth, hidden_half), jnp.bfloat16),
+            held(first),
+            held(hidden_half),
+            held(hidden_half),
+            held(hidden_half),
             pltpu.VMEM((8,) + block, jnp.bfloat16),
             pltpu.VMEM((8,) + block, jnp.bfloat16),
             pltpu.VMEM((8,) + block, jnp.bfloat16),
@@ -606,30 +709,18 @@
             pltpu.SemaphoreType.DMA((2, 7)),
             pltpu.SemaphoreType.DMA((2, 8)),
             pltpu.SemaphoreType.DMA((2,)),
-            pltpu.SemaphoreType.DMA((2, 7)),
-            pltpu.SemaphoreType.DMA((2, 7)),
+            pltpu.SemaphoreType.DMA((2, 10)),
+            pltpu.SemaphoreType.DMA((2, 10)),
             pltpu.VMEM((2, rows, hidden_half), jnp.float32),
             pltpu.VMEM((2, rows, hidden_half), jnp.bfloat16),
             pltpu.VMEM(block, jnp.bfloat16),
+            pltpu.VMEM((6, rows // 2, width), jnp.bfloat16),
         ],
         compiler_params=pltpu.CompilerParams(
             collective_id=0, has_side_effects=True, vmem_limit_bytes=60 * 1024 * 1024
         ),
         name="layer",
-    )(
-        tokens,
-        norm_in_gain.reshape(1, -1),
-        norm_mid_gain.reshape(1, -1),
-        wa,
-        wg,
-        wv,
-        wd,
-        taps,
-        bias,
-        jnp.asarray(cosine),
-        jnp.asarray(sine),
-        jnp.asarray(turn, jnp.bfloat16),
-    )
+    )(*operands)
 
 
 def solution(mesh):

time: 135 us -> 102 us (0.76)
  Pallas kernels: 123 us -> 98.2 us
  local copies, waits for them, and re-layouts: 8.96 us -> 3.61 us
  other arithmetic: 3.27 us -> 0 us
    pallas_call x1, Pallas kernels: 123 us -> 98.2 us  [fused(): pl.pallas_call(lambda *refs: layer_kernel(fs_count, heads, *refs), out_sh...]
    another operation x4 -> x0, other arithmetic: 3.19 us -> none  [the longest x1 0.96 us: fused(): wg = jnp.stack([up_gate_w[:, :hidden_half], up_gate_w[:, hidden_half:]])]
    unnamed x29 -> x2, local copies, waits for them, and re-layouts: 6.21 us -> 3.61 us
where the time goes in v2:
time: 102 us
  Pallas kernels  98.2 us (96%)
  local copies, waits for them, and re-layouts  3.61 us (4%)
    pallas_call x1, Pallas kernels, fused(): pl.pallas_call(lambda *refs: layer_kernel(fs_count, heads, *refs), out_sh...  98.2 us
    unnamed x2, local copies, waits for them, and re-layouts  3.61 us

profile of v2, /device:TPU:0, one launch (start us, length us, event | category | flops | bytes accessed | tf_op | source)
XLA Modules:
  0.0 101.9 jit_solution(13037676999382831691)
XLA Ops:
  0.0 2.0 %copy.17.refs_8_ = bf16[1024,192]{1,0:T(8,128)(2,1)} copy(bf16[1024,192]{0,1:T(8,128)(2,1)} %param.28) | data formatting | bytes 786432 | tf_op args[12]
  2.0 98.2 %layer.1 = bf16[256,384]{1,0:T(8,128)(2,1)} custom-call(bf16[256,384]{1,0:T(8,128)(2,1)} %refs_0_.1, bf16[192,192]{1,0:T(8,128)(2,1)} %refs_1_.1, bf16[192,192]{1,0:T(8,128)(2,1)} %refs_2_.1, bf16[192,192]{1,0:T(8,128)(2,1)} %refs_3_.1, bf16[192,192]{1,0:T(8,128)(2,1)} %refs_4_.1, bf16[192,192]{1,0:T(8,128)(2,1)} %refs_5_.1, bf16[192,1024]{1,0:T(8,128)(2,1)} %refs_6_.1, ...), custom_call_target="tpu_custom_call" | custom-call | tf_op jit(solution)/shard_map/layer/pallas_call | solution.py:685
  100.2 1.6 %copy.19 = bf16[256,384]{1,0:T(8,128)(2,1)} copy(bf16[256,384]{1,0:T(8,128)(2,1)} %layer.1) | data formatting | bytes 393216
